TPU v7x, 128 devices: a whole 4x4x4 slice. The times are simulated.
128 devices in a mesh: sp: 32 (over z, y, core), tp: 4 (over x).
Axes of the slice: x: 4, y: 4, z: 4, core: 2. Of those that a mesh axis runs over, the one named last changes fastest.
Arguments:
- residual: bfloat16 [32768, 2048], P('sp'), may hold values from -8 to 8
- query_wide: bfloat16 [32768, 1024], P('sp', 'tp'), may hold values from -6 to 6
- key_wide: bfloat16 [32768, 1024], P('sp', 'tp'), may hold values from -6 to 6
- value_wide: bfloat16 [32768, 2048], P('sp', 'tp'), may hold values from -6 to 6
- decay_wide: bfloat16 [32768, 1024], P('sp', 'tp'), may hold values from -12 to 12
- gate_wide: bfloat16 [32768, 2048], P('sp', 'tp'), may hold values from -6 to 6
- query_narrow: bfloat16 [32768, 512], P('sp', 'tp'), may hold values from -6 to 6
- key_narrow: bfloat16 [32768, 512], P('sp', 'tp'), may hold values from -6 to 6
- value_narrow: bfloat16 [32768, 2048], P('sp', 'tp'), may hold values from -6 to 6
- decay_narrow: bfloat16 [32768, 512], P('sp', 'tp'), may hold values from -12 to 12
- gate_narrow: bfloat16 [32768, 2048], P('sp', 'tp'), may hold values from -6 to 6
- head_gain: float32 [512], replicated, may hold values from 0.1 to 1.9
- out_wide: bfloat16 [2048, 2048], P('tp'), may hold values from -0.125 to 0.125
- out_narrow: bfloat16 [2048, 2048], P('tp'), may hold values from -0.125 to 0.125
- mlp_gain: float32 [2048], replicated, may hold values from 0.1 to 1.9
- up_weight: bfloat16 [2048, 4096], P('sp', 'tp'), may hold values from -0.125 to 0.125
- down_weight: bfloat16 [4096, 2048], P('tp', 'sp'), may hold values from -0.09375 to 0.09375
Outputs:
- layer_out: bfloat16 [32768, 2048], P('sp', 'tp')
All inputs are finite; a program needn't handle non-finite values.
Results may differ from a plain program's by a relative error of at most 0.017.
Values may be sent and summed in bfloat16 or wider, within the bound.
No kernel may reach another device: no remote copies, remote signals or barrier semaphores. Data moves between devices by JAX's collectives and lax.ppermute only.
A program may use at most 128 MiB of HBM per device.

v0:
```python
import jax
import jax.numpy as jnp
from jax import lax
from jax.sharding import PartitionSpec as P

HEADS = 4
BLOCK = 64


EPS = 1e-05
DECAY_NORMALIZER = 16.0
HIGHEST = lax.Precision.HIGHEST


def turned_gather(arrays, axis, dims):
    turned = [jnp.moveaxis(a, dim, 0) for a, dim in zip(arrays, dims)]
    both = jnp.concatenate([t.reshape(len(t), -1) for t in turned], axis=1)
    whole, at, finished = (lax.all_gather(both, axis, axis=0, tiled=True), 0, [])
    for t, dim in zip(turned, dims):
        section = whole[:, at : at + t[0].size].reshape(-1, *t.shape[1:])
        finished.append(jnp.moveaxis(section, 0, dim))
        at += t[0].size
    return tuple(finished)


def entering(array, axis, join, neutral):
    place = lax.axis_index(axis)
    gathered = jax.tree.map(
        lambda a, kind: lax.all_gather(a.astype(kind), axis),
        array,
        (jnp.bfloat16, jnp.bfloat16, jnp.bfloat16, jnp.bfloat16),
    )
    state = jax.tree.map(lambda a, e: jnp.zeros_like(a) + jnp.asarray(e, a.dtype), array, neutral)

    def one(step, state):
        return join(
            state,
            jax.tree.map(
                lambda a, own: lax.dynamic_index_in_dim(a, step, 0, False).astype(own.dtype),
                gathered,
                array,
            ),
        )

    return lax.fori_loop(0, place, one, state)


def split_up(array, dim, count):
    dims = array.shape
    pieces = array.reshape(*dims[:dim], count, dims[dim] // count, *dims[dim + 1 :])
    return jnp.moveaxis(pieces, dim, 0)


def sum_at_owner(array, axis, dim):
    count = lax.axis_size(axis)
    pieces = lax.all_to_all(split_up(array, dim, count), axis, 0, 0, tiled=True)
    return jnp.sum(pieces.astype(jnp.float32), axis=0)


def sent_to_all(array, axis):
    copies = jnp.broadcast_to(array, (lax.axis_size(axis), *array.shape))
    return lax.all_to_all(copies, axis, split_axis=0, concat_axis=0, tiled=True)


def of_everyone(array, axis):
    everything = sent_to_all(array, axis)
    return jnp.sum(everything, axis=0)


def block_pass(queries, keys_in, values_in, log_decay, block_len):
    num_blocks = queries.shape[0] // block_len

    def to_blocks(stacked):
        return stacked.reshape((num_blocks, block_len) + stacked.shape[1:])

    causal = jnp.tril(jnp.ones((block_len, block_len), dtype=bool))
    initial = (
        jnp.zeros((queries.shape[1], queries.shape[2], values_in.shape[2]), jnp.float32),
        jnp.zeros((queries.shape[1], queries.shape[2]), jnp.float32),
    )

    def advance(running, inputs):
        memory, offset = running
        block_q, block_k, block_v, block_g = inputs
        within = jnp.cumsum(block_g, axis=0)
        final_log = within[-1]
        scaled_q = block_q * jnp.exp(within)
        scaled_k = block_k * jnp.exp(-within)
        outside = jnp.einsum("ihd,hde->ihe", scaled_q, memory, precision=HIGHEST)
        scores = jnp.einsum("ihd,jhd->hij", scaled_q, scaled_k, precision=HIGHEST)
        scores = jnp.where(causal[None], scores, 0.0)
        inside = jnp.einsum("hij,jhe->ihe", scores, block_v, precision=HIGHEST)
        decayed_keys = scaled_k * jnp.exp(final_log)[None]
        memory = jnp.exp(final_log)[..., None] * memory + jnp.einsum(
            "jhd,jhe->hde", decayed_keys, block_v, precision=HIGHEST
        )
        carried_q = scaled_q * jnp.exp(offset)[None]
        return ((memory, offset + final_log), (outside + inside, carried_q))

    (memory, totals), (outputs, carried_q) = lax.scan(
        advance,
        initial,
        (to_blocks(queries), to_blocks(keys_in), to_blocks(values_in), to_blocks(log_decay)),
    )
    return (outputs.reshape(values_in.shape), carried_q.reshape(queries.shape), totals, memory)


def prepare(query, key_proj, value, decay, heads_here):
    row_count = query.shape[0]
    key_width = query.shape[1] // heads_here
    queries = query.astype(jnp.float32).reshape(row_count, heads_here, key_width) * key_width ** (
        -0.5
    )
    keys_in = key_proj.astype(jnp.float32).reshape(row_count, heads_here, key_width)
    values_in = value.astype(jnp.float32).reshape(
        row_count, heads_here, value.shape[1] // heads_here
    )
    log_decay = (
        jax.nn.log_sigmoid(decay.astype(jnp.float32)).reshape(row_count, heads_here, key_width)
        / DECAY_NORMALIZER
    )
    return (queries, keys_in, values_in, log_decay)


def finish(outputs, gate, head_gain):
    scale = lax.rsqrt(jnp.mean(jnp.square(outputs), axis=-1, keepdims=True) + EPS)
    gated = (
        outputs * scale * head_gain * jax.nn.silu(gate.astype(jnp.float32).reshape(outputs.shape))
    )
    return gated.reshape(outputs.shape[0], -1).astype(jnp.bfloat16)


def combine_states(earlier, later):
    return (
        earlier[0] + later[0],
        jnp.exp(later[0])[..., None] * earlier[1] + later[1],
        earlier[2] + later[2],
        jnp.exp(later[2])[..., None] * earlier[3] + later[3],
    )


def body(
    residual,
    query_wide,
    key_wide,
    value_wide,
    decay_wide,
    gate_wide,
    query_narrow,
    key_narrow,
    value_narrow,
    decay_narrow,
    gate_narrow,
    head_gain,
    out_wide,
    out_narrow,
    mlp_gain,
    up_weight,
    down_weight,
):
    heads_here = HEADS // lax.axis_size("tp")
    up_whole, down_whole = turned_gather((up_weight, down_weight), "sp", (0, 1))
    wq, wk, wv, wg = prepare(query_wide, key_wide, value_wide, decay_wide, heads_here)
    wide_out, wide_q, wide_total, wide_memory = block_pass(wq, wk, wv, wg, BLOCK)
    nq, nk, nv, ng = prepare(query_narrow, key_narrow, value_narrow, decay_narrow, heads_here)
    narrow_out, narrow_q, narrow_total, narrow_memory = block_pass(nq, nk, nv, ng, BLOCK)
    identity = (
        jnp.zeros_like(wide_total),
        jnp.zeros_like(wide_memory),
        jnp.zeros_like(narrow_total),
        jnp.zeros_like(narrow_memory),
    )
    incoming = entering(
        (wide_total, wide_memory, narrow_total, narrow_memory), "sp", combine_states, identity
    )
    wide_out = wide_out + jnp.einsum("ihd,hde->ihe", wide_q, incoming[1], precision=HIGHEST)
    narrow_out = narrow_out + jnp.einsum("ihd,hde->ihe", narrow_q, incoming[3], precision=HIGHEST)
    gated_wide = finish(wide_out, gate_wide, head_gain)
    gated_narrow = finish(narrow_out, gate_narrow, head_gain)
    head_terms = jnp.dot(gated_wide, out_wide, preferred_element_type=jnp.float32) + jnp.dot(
        gated_narrow, out_narrow, preferred_element_type=jnp.float32
    )
    tp_index = lax.axis_index("tp")
    col_count = residual.shape[1] // lax.axis_size("tp")
    full_width = residual.shape[1]
    residual_cols = lax.dynamic_slice_in_dim(residual, tp_index * col_count, col_count, 1)
    mixed_cols = sum_at_owner(head_terms.astype(jnp.bfloat16), "tp", 1)
    stream_cols = (residual_cols.astype(jnp.float32) + mixed_cols).astype(jnp.bfloat16)
    stream_f = stream_cols.astype(jnp.float32)
    squares = of_everyone(jnp.sum(jnp.square(stream_f), axis=1, keepdims=True), "tp")
    gain_cols = lax.dynamic_slice_in_dim(mlp_gain, tp_index * col_count, col_count, 0)
    normed_cols = (stream_f * lax.rsqrt(squares / full_width + EPS) * gain_cols).astype(
        jnp.bfloat16
    )
    normed = lax.all_gather(normed_cols, "tp", axis=1, tiled=True)
    before_activation = jnp.dot(normed, up_whole, preferred_element_type=jnp.float32)
    hidden = jnp.square(jax.nn.relu(before_activation)).astype(jnp.bfloat16)
    down_terms = jnp.dot(hidden, down_whole, preferred_element_type=jnp.float32)
    mlp_cols = sum_at_owner(down_terms.astype(jnp.bfloat16), "tp", 1)
    return (stream_cols.astype(jnp.float32) + mlp_cols).astype(jnp.bfloat16)


def solution(mesh):
    return jax.shard_map(
        body,
        mesh=mesh,
        in_specs=(
            P("sp", None),
            P("sp", "tp"),
            P("sp", "tp"),
            P("sp", "tp"),
            P("sp", "tp"),
            P("sp", "tp"),
            P("sp", "tp"),
            P("sp", "tp"),
            P("sp", "tp"),
            P("sp", "tp"),
            P("sp", "tp"),
            P(),
            P("tp", None),
            P("tp", None),
            P(),
            P("sp", "tp"),
            P("tp", "sp"),
        ),
        out_specs=P("sp", "tp"),
        check_vma=False,
    )
```

profile of v0, /device:TPU:0, one launch (start us, length us, event | category | flops | bytes accessed | tf_op | source)
XLA Modules:
  0.0 539.1 jit_solution(10759921777863404328)
XLA Ops:
  6.6 5.0 reshape.518
  15.4 68.4 %while.51 = (s32[]{:T(128)}, f32[1,128,512]{2,1,0:T(8,128)S(1)}, f32[1,128]{1,0:T(1,128)S(1)}, f32[16,64,1,512]{3,1,2,0:T(8,128)}, f32[16,64,1,128]{3,1,2,0:T(8,...) while((s32[]{:T(128)}, f32[1,128,512]{2,1,0:T(8,128)S(1)}, ...), condition=%wide.region_5.6_spmd.clone, body=%wide.region_3.5_spmd.clone.sunk | while | flops 133005568 | bytes 2333321 | solution.py:100
  84.7 2.7 fusion.90
  87.3 3.3 reshape.501
  91.6 3.4 reshape.502
  95.0 4.9 reshape.516
  103.5 108.8 %while.50 = (s32[]{:T(128)}, f32[1,256,512]{2,1,0:T(8,128)S(1)}, f32[1,256]{1,0:T(1,128)S(1)}, f32[16,64,1,512]{3,1,2,0:T(8,128)}, f32[16,64,1,256]{3,1,2,0:T(8,...) while((s32[]{:T(128)}, f32[1,256,512]{2,1,0:T(8,128)S(1)}, ...), condition=%wide.region_2.3_spmd.clone, body=%wide.region_0.2_spmd.clone.sunk | while | flops 240787968 | bytes 3648133 | solution.py:100
  213.9 3.0 copy.32
  218.2 3.0 copy.34
  222.6 23.1 %all-gather.5 = bf16[32,1,128]{2,1,0:T(2,128)(2,1)S(1)} all-gather(bf16[1,1,128]{2,1,0:T(2,128)(2,1)S(1)} %convert_bitcast_fusion.1), channel_id=4, replica_groups=mesh['sp'=32,'tp'=4] {'sp'}, dimensions={0}, use_global_device_ids=true | all-gather | bytes 8448 | tf_op jit(solution)/shard_map/all_gather | solution.py:29
  245.7 23.8 %all-gather.4 = bf16[32,1,256]{2,1,0:T(2,128)(2,1)S(1)} all-gather(bf16[1,1,256]{2,1,0:T(2,128)(2,1)S(1)} %convert_bitcast_fusion), channel_id=2, replica_groups=mesh['sp'=32,'tp'=4] {'sp'}, dimensions={0}, use_global_device_ids=true | all-gather | bytes 16896 | tf_op jit(solution)/shard_map/all_gather | solution.py:29
  269.6 5.6 %multiply_reduce_fusion.1 = (f32[1024]{0:T(1024)S(1)}, f32[1024,1,512]{0,2,1:T(8,128)S(1)}) fusion(f32[1024,1,512]{0,2,1:T(8,128)} %copy.32, f32[1024,256]{1,0:T(8,128)} %bitcast.301, f32[1,256,512]{2,1,0:T(8,128)S(1)} %get-tuple-element.190), kind=kOutput, calls=%fused_computation.128 | convolution fusion | flops 1612184576 | bytes 5771264 | tf_op jit(solution)/shard_map/ihd,hde->ihe/dot_general | solution.py:176
  277.4 2.8 fusion.87
  280.2 3.1 add_convert_fusion
  283.3 2.2 copy.90
  285.5 5.1 all-to-all-start
  290.7 48.5 %all-to-all-done = bf16[4,1024,512]{2,1,0:T(8,128)(2,1)} async-done(((bf16[4,1024,512]{2,1,0:T(8,128)(2,1)}), bf16[4,1024,512]{2,1,0:T(8,128)(2,1)}, u32[]{:S(2)}, u32[]{:S(2)}) %all-to-all-start) | async-done | bytes 4194336 | tf_op jit(solution)/shard_map/all_to_all | solution.py:56
  339.1 3.0 convert_reduce_fusion.1
  344.4 3.3 all-to-all-start.1
  348.5 4.5 all-to-all-done.1
  354.4 111.0 %all-gather.11.cloned.1.call-done = bf16[1024,2048]{1,0:T(8,128)(2,1)} async-done(((bf16[1024,512]{1,0:T(8,128)(2,1)}), bf16[1024,2048]{1,0:T(8,128)(2,1)}) %all-gather.11.cloned.1.call-update) | async-done | bytes 4194320 | tf_op jit(solution)/shard_map/all_gather | solution.py:195
  465.4 8.1 %multiply_convert_fusion = bf16[1024,1024]{1,0:T(8,128)(2,1)S(1)} fusion(bf16[1024,2048]{1,0:T(8,128)(2,1)} %all-gather.11.cloned.1.call-done, bf16[2048,2048]{1,0:T(8,128)(2,1)} %all-gather.13.cloned.1.call-done), kind=kOutput, calls=%fused_computation.98 | convolution fusion | flops 4298113024 | bytes 10485760 | tf_op jit(solution)/shard_map/dot_general | solution.py:196
  473.5 4.8 fusion.63
  478.7 51.8 %all_to_all.15 = bf16[4,1024,512]{2,1,0:T(8,128)(2,1)S(1)} all-to-all(bf16[4,1024,512]{2,1,0:T(8,128)(2,1)S(1)} %bitcast.288), channel_id=1, replica_groups=mesh['sp'=32,'tp'=4] {'tp'}, dimensions={0} | all-to-all | bytes 8388608 | tf_op jit(solution)/shard_map/all_to_all | solution.py:56
  (432 shorter events, 198.1 us)
Async XLA Ops:
  6.5 270.8 %copy-start = (bf16[512,2048]{1,0:T(8,128)(2,1)S(1)}, bf16[512,2048]{1,0:T(8,128)(2,1)}, u32[]{:S(2)}) copy-start(bf16[512,2048]{1,0:T(8,128)(2,1)} %param.35) | copy-start | bytes 6291460
  6.5 5.1 copy-start.10
  6.5 5.1 copy-start.11
  6.5 263.0 %all-gather.17.cloned.1.call-start = ((), (), s32[]{:S(2)}) async-start(), calls=%async_computation.6 | async-start | bytes 4325376 | tf_op jit(solution)/shard_map/all_gather | solution.py:29
  83.9 6.7 %copy-start.7 = (bf16[1024,256]{1,0:T(8,128)(2,1)S(1)}, bf16[1024,256]{1,0:T(8,128)(2,1)}, u32[]{:S(2)}) copy-start(bf16[1024,256]{1,0:T(8,128)(2,1)} %param.24) | copy-start | bytes 1572868
  84.6 184.9 %all-gather.15.cloned.1.call-start = ((), (), s32[]{:S(2)}) async-start(), calls=%async_computation.5 | async-start | bytes 8650752 | tf_op jit(solution)/shard_map/all_gather | solution.py:29
  91.6 8.2 %copy-start.8 = (bf16[1024,256]{1,0:T(8,128)(2,1)S(1)}, bf16[1024,256]{1,0:T(8,128)(2,1)}, u32[]{:S(2)}) copy-start(bf16[1024,256]{1,0:T(8,128)(2,1)} %param.25) | copy-start | bytes 1572868
  103.5 109.6 %copy-start.12 = (bf16[1024,64]{0,1:T(8,128)(2,1)S(1)}, bf16[1024,64]{0,1:T(8,128)(2,1)}, u32[]{:S(2)}) copy-start(bf16[1024,64]{0,1:T(8,128)(2,1)} %param.39) | copy-start | bytes 393220
  103.5 109.6 %copy-start.13 = (bf16[64,1024]{1,0:T(8,128)(2,1)S(1)}, bf16[64,1024]{1,0:T(8,128)(2,1)}, u32[]{:S(2)}) copy-start(bf16[64,1024]{1,0:T(8,128)(2,1)} %param.38) | copy-start | bytes 393220
  213.1 141.3 %all-gather.13.cloned.1.call-start = ((), (), s32[]{:S(2)}) async-start(), calls=%async_computation.4 | async-start | bytes 8650752 | tf_op jit(solution)/shard_map/all_gather | solution.py:18
  213.9 3.0 copy-start.3
  218.2 3.0 copy-start.4
  269.6 5.7 %copy-start.2 = (f32[1024,1,512]{0,2,1:T(8,128)S(1)}, f32[1024,1,512]{0,2,1:T(8,128)}, u32[]{:S(2)}) copy-start(f32[1024,1,512]{0,2,1:T(8,128)} %copy.34) | copy-start | bytes 6291460
  269.6 5.7 %copy-start.9 = (f32[16,64,1,128]{3,1,2,0:T(8,128)S(1)}, f32[16,64,1,128]{3,1,2,0:T(8,128)}, u32[]{:S(2)}) copy-start(f32[16,64,1,128]{3,1,2,0:T(8,128)} %get-tuple-element.194) | copy-start | bytes 1572868
  275.3 2.1 copy-start.6
  275.3 2.1 copy-start.16
  277.4 2.8 copy-start.5
  277.4 2.8 copy-start.15
  285.5 53.6 %all-to-all-start = ((bf16[4,1024,512]{2,1,0:T(8,128)(2,1)}), bf16[4,1024,512]{2,1,0:T(8,128)(2,1)}, u32[]{:S(2)}, u32[]{:S(2)}) async-start(bf16[4,1024,512]{2,1,0:T(8,128)(2,1)} %bitcast.287), calls=%async_computation | async-start | bytes 8388608 | tf_op jit(solution)/shard_map/all_to_all | solution.py:56
  344.4 8.6 %all-to-all-start.1 = ((f32[4,1024,1]{1,2,0:T(1,128)}), f32[4,1024,1]{1,2,0:T(1,128)S(1)}, u32[]{:S(2)}, u32[]{:S(2)}) async-start(f32[4,1024,1]{1,2,0:T(1,128)} %broadcast_in_dim.50), calls=%async_computation.1 | async-start | bytes 32768 | tf_op jit(solution)/shard_map/all_to_all | solution.py:62
  347.7 117.7 %all-gather.11.cloned.1.call-start = ((), (), s32[]{:S(2)}) async-start(), calls=%async_computation.3 | async-start | bytes 5242880 | tf_op jit(solution)/shard_map/all_gather | solution.py:195
  465.4 8.1 %copy-start.14 = (bf16[2048,2048]{1,0:T(8,128)(2,1)S(1)}, bf16[2048,2048]{1,0:T(8,128)(2,1)}, u32[]{:S(2)}) copy-start(bf16[2048,2048]{1,0:T(8,128)(2,1)} %all-gather.13.cloned.1.call-done) | copy-start | bytes 25165828
  530.4 2.1 copy-start.1
Sparse Core Ops, SparseCore 0:
  84.7 48.7 all-gather.16
  213.2 55.4 all-gather.14
  271.0 52.3 all-gather.12
  354.5 110.8 all-gather.10
where the time goes:
time: 545 us; the launch traced here: 539 us
  waiting for transfers between devices  164 us (30%)
  blocking collectives  98.6 us (18%)
  matrix products  91.9 us (17%)
  local copies, waits for them, and re-layouts  86.4 us (16%)
  other arithmetic  74.3 us (14%)
  between operations  13.5 us (2%)
  starting transfers between devices  8.53 us (2%)
    all_gather x1, waiting for transfers between devices, body(): normed = lax.all_gather(normed_cols, 'tp', axis=1, tiled=True)  111 us
    all_to_all x1, blocking collectives, sum_at_owner(): pieces = lax.all_to_all(split_up(array, dim, count), axis, 0, 0, tiled=True)  51.8 us
    all_to_all x1, waiting for transfers between devices, sum_at_owner(): pieces = lax.all_to_all(split_up(array, dim, count), axis, 0, 0, tiled=True)  48.5 us
    all_gather x2, blocking collectives, entering(): lax.all_gather(a.astype(kind), axis)  46.9 us
    dynamic_slice x48, local copies, waits for them, and re-layouts, block_pass(): lax.scan(advance, initial, (to_blocks(queries), to_blocks(keys_in), to_bl...  41.7 us
    dot_general x32, matrix products, advance(): outside = jnp.einsum('ihd,hde->ihe', scaled_q, memory, precision=HIGHEST)  22.1 us
    dot_general x32, matrix products, advance(): inside = jnp.einsum('hij,jhe->ihe', scores, block_v, precision=HIGHEST)  19.3 us
    dot_general x32, matrix products, advance(): jnp.einsum('jhd,jhe->hde', decayed_keys, block_v, precision=HIGHEST)  17.8 us
  transfers between devices with their start and end apart: 6, of which 3 were waited for; matrix products, arithmetic and copies ran while one was open for 30% of the time, Pallas kernels for 0%

commit v1 on v0

v1 whole, which is shorter than its diff:
```python
import functools

import jax
import jax.numpy as jnp
from jax import lax
from jax.experimental import pallas as pl
from jax.experimental.pallas import tpu as pltpu
from jax.sharding import PartitionSpec as P

EPS = 1e-05
DECAY_NORMALIZER = 16.0
CHUNK = 128
F32 = jnp.float32
BF16 = jnp.bfloat16
NT = (((1,), (1,)), ((), ()))
TN = (((0,), (0,)), ((), ()))
E_ROWS = 8


def dot(a, b, dims=(((1,), (0,)), ((), ()))):
    return lax.dot_general(a, b, dims, preferred_element_type=F32)


def log_decay_of(pre):
    x = pre.astype(F32)
    return (jnp.minimum(x, 0.0) - jnp.log1p(jnp.exp(-jnp.abs(x)))) / DECAY_NORMALIZER


def tri_sum(tri, g):
    high = g.astype(BF16)
    low = (g - high.astype(F32)).astype(BF16)
    return dot(tri, high) + dot(tri, low)


def tri_mask(kind):
    row = lax.broadcasted_iota(jnp.int32, (CHUNK, CHUNK), 0)
    col = lax.broadcasted_iota(jnp.int32, (CHUNK, CHUNK), 1)
    return (col <= row) if kind == "lower" else (col > row)


def params(**kw):
    return pltpu.CompilerParams(vmem_limit_bytes=56 * 1024 * 1024, **kw)


def state_kernel(kw, dw, vw, kn, dn, vn, packed, decayed_w, decayed_n):
    later = tri_mask("upper").astype(BF16)
    rows = kw.shape[0]
    keys_w = kw.shape[1]
    for key, pre, decayed, value, at in (
        (kw, dw, decayed_w, vw, 0),
        (kn, dn, decayed_n, vn, keys_w),
    ):
        width = key.shape[1]
        offset = jnp.zeros((1, width), F32)
        for block in reversed(range(rows // CHUNK)):
            span = pl.ds(block * CHUNK, CHUNK)
            g = log_decay_of(pre[span, :])
            after = tri_sum(later, g)
            decayed[span, :] = (key[span, :].astype(F32) * jnp.exp(after + offset)).astype(BF16)
            offset = offset + after[0:1, :] + g[0:1, :]
        state = dot(value[...], decayed[...], TN)
        slices = packed.shape[0]
        state_rows = state.shape[0] // slices
        packed[:, 0:state_rows, at : at + width] = state.astype(BF16).reshape(
            slices, state_rows, width
        )
        packed[:, state_rows:, at : at + width] = jnp.broadcast_to(
            jnp.exp(offset).astype(BF16)[None], (slices, E_ROWS, width)
        )


def local_state(kw, dw, vw, kn, dn, vn, slices):
    rows, keys_w = kw.shape
    keys_n = kn.shape[1]
    state_rows = vw.shape[1] // slices
    return pl.pallas_call(
        state_kernel,
        out_shape=jax.ShapeDtypeStruct((slices, state_rows + E_ROWS, keys_w + keys_n), BF16),
        scratch_shapes=[pltpu.VMEM((rows, keys_w), BF16), pltpu.VMEM((rows, keys_n), BF16)],
        compiler_params=params(),
        name="local_state",
    )(kw, dw, vw, kn, dn, vn)


def scan_kernel(packed, entering):
    slices, state_rows, width = entering.shape
    state = jnp.zeros((state_rows, width), F32)
    for i in range(slices):
        entering[i] = state.astype(BF16)
        if i + 1 < slices:
            decay = packed[i, state_rows : state_rows + 1, :].astype(F32)
            state = state * decay + packed[i, 0:state_rows, :].astype(F32)


def scan_states(packed):
    slices, packed_rows, width = packed.shape
    return pl.pallas_call(
        scan_kernel,
        out_shape=jax.ShapeDtypeStruct((slices, packed_rows - E_ROWS, width), BF16),
        compiler_params=params(),
        name="scan_states",
    )(packed)


def intra_kernel(q, k, v, pre, out, carried, memory, offset):
    @pl.when(pl.program_id(0) == 0)
    def _():
        memory[...] = jnp.zeros_like(memory)
        offset[...] = jnp.zeros_like(offset)

    width = q.shape[1]
    lower = tri_mask("lower")
    g = log_decay_of(pre[...])
    within = tri_sum(lower.astype(BF16), g)
    final = within[CHUNK - 1 : CHUNK, :]
    middle = within[CHUNK // 2 : CHUNK // 2 + 1, :]
    queries = q[...].astype(F32) * width ** (-0.5)
    keys = k[...].astype(F32)
    values = v[...]
    near_q = (queries * jnp.exp(within - middle)).astype(BF16)
    near_k = (keys * jnp.exp(middle - within)).astype(BF16)
    scores = jnp.where(lower, dot(near_q, near_k, NT), 0.0).astype(BF16)
    decayed_q = queries * jnp.exp(within)
    held = memory[...]
    outside = dot(decayed_q.astype(BF16), held.astype(BF16), NT)
    out[...] = outside + dot(scores, values)
    carried[...] = (decayed_q * jnp.exp(offset[...])).astype(BF16)
    offset[...] = offset[...] + final
    decayed_k = (keys * jnp.exp(final - within)).astype(BF16)
    memory[...] = held * jnp.exp(final) + dot(values, decayed_k, TN)


def intra(q, k, v, pre, name):
    rows, width = q.shape
    value_width = v.shape[1]

    def spec(cols):
        return pl.BlockSpec((CHUNK, cols), lambda i: (i, 0))

    return pl.pallas_call(
        intra_kernel,
        grid=(rows // CHUNK,),
        in_specs=[spec(width), spec(width), spec(value_width), spec(width)],
        out_specs=[spec(value_width), spec(width)],
        out_shape=[
            jax.ShapeDtypeStruct((rows, value_width), F32),
            jax.ShapeDtypeStruct((rows, width), BF16),
        ],
        scratch_shapes=[pltpu.VMEM((value_width, width), F32), pltpu.VMEM((1, width), F32)],
        compiler_params=params(dimension_semantics=("arbitrary",)),
        name=name,
    )(q, k, v, pre)


def project_kernel(aw, cw, gw, an, cn, gn, state, gain, ow, on, out):
    keys_w = cw.shape[1]

    def gated(inside, carried, gate, held):
        att = inside[...] + dot(carried[...], held, NT)
        scale = lax.rsqrt(jnp.mean(jnp.square(att), axis=-1, keepdims=True) + EPS)
        u = gate[...].astype(F32)
        return (att * scale * gain[...] * (u / (1.0 + jnp.exp(-u)))).astype(BF16)

    wide = gated(aw, cw, gw, state[:, :keys_w])
    narrow = gated(an, cn, gn, state[:, keys_w:])
    out[...] = (dot(wide, ow[...]) + dot(narrow, on[...])).astype(BF16)


def project(aw, cw, gw, an, cn, gn, state, gain, ow, on, blocks):
    rows = aw.shape[0]
    step = rows // blocks
    full = ow.shape[1]

    def spec(a):
        return pl.BlockSpec((step, a.shape[1]), lambda i: (i, 0))

    def whole(a):
        return pl.BlockSpec(a.shape, lambda i: (0, 0))

    return pl.pallas_call(
        project_kernel,
        grid=(blocks,),
        in_specs=[spec(a) for a in (aw, cw, gw, an, cn, gn)]
        + [whole(a) for a in (state, gain, ow, on)],
        out_specs=pl.BlockSpec((step, full), lambda i: (i, 0)),
        out_shape=jax.ShapeDtypeStruct((rows, full), BF16),
        compiler_params=params(dimension_semantics=("arbitrary",)),
        name="project",
    )(aw, cw, gw, an, cn, gn, state, gain, ow, on)


def stream_kernel(place, parts, residual, gain, stream, normed):
    total = residual[...].astype(F32)
    mixed = parts[0].astype(F32)
    for i in range(1, parts.shape[0]):
        mixed = mixed + parts[i].astype(F32)
    held = (total + mixed).astype(BF16)
    stream[...] = held
    wide = held.astype(F32)
    scale = lax.rsqrt(jnp.mean(jnp.square(wide), axis=-1, keepdims=True) + EPS)
    normed[...] = (wide * scale * gain[...]).astype(BF16)


def make_stream(place, parts, residual, gain):
    count, rows, full = parts.shape
    return pl.pallas_call(
        stream_kernel,
        grid_spec=pltpu.PrefetchScalarGridSpec(
            num_scalar_prefetch=1,
            grid=(1,),
            in_specs=[
                pl.BlockSpec((count, rows, full), lambda i, p: (0, 0, 0)),
                pl.BlockSpec((rows, full), lambda i, p: (p[0], 0)),
                pl.BlockSpec((1, full), lambda i, p: (0, 0)),
            ],
            out_specs=[
                pl.BlockSpec((rows, full), lambda i, p: (0, 0)),
                pl.BlockSpec((rows, full), lambda i, p: (0, 0)),
            ],
        ),
        out_shape=[jax.ShapeDtypeStruct((rows, full), BF16)] * 2,
        compiler_params=params(dimension_semantics=("arbitrary",)),
        name="make_stream",
    )(place, parts, residual, gain)


def mixer_kernel(normed, stream, up, down, out, total):
    step = pl.program_id(0)
    full = normed.shape[1]
    width = up.shape[-1]
    before = dot(normed[...], up[...].reshape(full, width))
    hidden = jnp.square(jnp.maximum(before, 0.0)).astype(BF16)
    term = dot(hidden, down[...].reshape(full, width), NT)

    @pl.when(step == 0)
    def _():
        total[...] = term

    @pl.when(step > 0)
    def _():
        total[...] = total[...] + term

    @pl.when(step == pl.num_programs(0) - 1)
    def _():
        cols = out.shape[2]
        for i in range(out.shape[0]):
            span = slice(i * cols, (i + 1) * cols)
            out[i] = (stream[:, span].astype(F32) + total[:, span]).astype(BF16)


def mixer(normed, stream, weights, count, width):
    rows, full = normed.shape
    n_sp, n_tp, both, cols = weights.shape
    per = cols // width

    def at(half):
        return pl.BlockSpec(
            (n_sp, 1, both // 2, width), lambda s: (0, s // per, half, s % per)
        )

    return pl.pallas_call(
        mixer_kernel,
        grid=(n_tp * per,),
        in_specs=[
            pl.BlockSpec((rows, full), lambda s: (0, 0)),
            pl.BlockSpec((rows, full), lambda s: (0, 0)),
            at(0),
            at(1),
        ],
        out_specs=pl.BlockSpec((count, rows, full // count), lambda s: (0, 0, 0)),
        out_shape=jax.ShapeDtypeStruct((count, rows, full // count), BF16),
        scratch_shapes=[pltpu.VMEM((rows, full), F32)],
        compiler_params=params(dimension_semantics=("arbitrary",)),
        name="mixer",
    )(normed, stream, weights, weights)


def body(
    residual,
    query_wide,
    key_wide,
    value_wide,
    decay_wide,
    gate_wide,
    query_narrow,
    key_narrow,
    value_narrow,
    decay_narrow,
    gate_narrow,
    head_gain,
    out_wide,
    out_narrow,
    mlp_gain,
    up_weight,
    down_weight,
):
    n_sp = lax.axis_size("sp")
    n_tp = lax.axis_size("tp")
    rows, full = residual.shape
    own = jnp.concatenate((up_weight, down_weight.T), axis=0)
    weights = lax.all_gather(own, ("sp", "tp"), axis=0, tiled=False)
    weights = weights.reshape(n_sp, n_tp, *own.shape)
    packed = local_state(
        key_wide, decay_wide, value_wide, key_narrow, decay_narrow, value_narrow, n_sp
    )
    packed = lax.all_to_all(packed, "sp", 0, 0, tiled=True)
    wide_in, wide_q = intra(query_wide, key_wide, value_wide, decay_wide, "intra_wide")
    narrow_in, narrow_q = intra(
        query_narrow, key_narrow, value_narrow, decay_narrow, "intra_narrow"
    )
    entering = lax.all_to_all(scan_states(packed), "sp", 0, 0, tiled=True)
    state = entering.reshape(-1, entering.shape[2])
    terms = project(
        wide_in,
        wide_q,
        gate_wide,
        narrow_in,
        narrow_q,
        gate_narrow,
        state,
        head_gain.reshape(1, -1),
        out_wide,
        out_narrow,
        n_tp,
    )
    parts = lax.all_to_all(terms.reshape(n_tp, rows // n_tp, full), "tp", 0, 0, tiled=True)
    place = lax.axis_index("tp").astype(jnp.int32).reshape(1)
    stream, normed = make_stream(place, parts, residual, mlp_gain.reshape(1, -1))
    finished = mixer(normed, stream, weights, n_tp, 512)
    sent = lax.all_to_all(finished, "tp", 0, 0, tiled=True)
    return sent.reshape(rows, full // n_tp)


def solution(mesh):
    return jax.shard_map(
        body,
        mesh=mesh,
        in_specs=(
            P("sp", None),
            P("sp", "tp"),
            P("sp", "tp"),
            P("sp", "tp"),
            P("sp", "tp"),
            P("sp", "tp"),
            P("sp", "tp"),
            P("sp", "tp"),
            P("sp", "tp"),
            P("sp", "tp"),
            P("sp", "tp"),
            P(),
            P("tp", None),
            P("tp", None),
            P(),
            P("sp", "tp"),
            P("tp", "sp"),
        ),
        out_specs=P("sp", "tp"),
        check_vma=False,
    )
```

time: 545 us -> 215 us (0.39)
  matrix products: 91.9 us -> 0 us
  local copies, waits for them, and re-layouts: 86.4 us -> 1.73 us
  waiting for transfers between devices: 164 us -> 88.3 us
  other arithmetic: 74.3 us -> 1.69 us
  Pallas kernels: 0 us -> 58.4 us
  blocking collectives: 98.6 us -> 41 us
    all_gather x4 -> x1, waiting for transfers between devices: 111 us -> 0.01 us  [body(): weights = lax.all_gather(own, ('sp', 'tp'), axis=0, tiled=False)]
    dot_general x134 -> x0, matrix products: 91.9 us -> none  [the longest x32 22.1 us: advance(): outside = jnp.einsum('ihd,hde->ihe', scaled_q, memory, precision=HIGHEST)]
    pallas_call x0 -> x7, Pallas kernels: none -> 58.4 us  [the longest x1 19 us: mixer(): pl.pallas_call(mixer_kernel, grid=(n_tp * per,), in_specs=[pl.BlockSpec((...]
    all_gather x2 -> x0, blocking collectives: 46.9 us -> none  [entering(): lax.all_gather(a.astype(kind), axis)]
    dynamic_slice x49 -> x0, local copies, waits for them, and re-layouts: 42.4 us -> none  [the longest x48 41.7 us: block_pass(): lax.scan(advance, initial, (to_blocks(queries), to_blocks(keys_in), to_bl...]
    all_to_all x2, waiting for transfers between devices: 53 us -> 88.3 us  [the longest x1 88.3 us: body(): lax.all_to_all(terms.reshape(n_tp, rows // n_tp, full), 'tp', 0, 0, tiled...]
    mul x34 -> x0, other arithmetic: 33.1 us -> none  [the longest x16 17 us: advance(): carried_q = scaled_q * jnp.exp(offset)[None]]
    another operation x33 -> x0, other arithmetic: 16.8 us -> none  [the longest x32 15.8 us: advance(): within = jnp.cumsum(block_g, axis=0)]
  transfers between devices with their start and end apart: 6 -> 3, of which waited for: 3 -> 1; matrix products, arithmetic and copies ran while one was open for 30% -> 0% of each run, Pallas kernels for 0% -> 18%
where the time goes in v1:
time: 215 us; the launch traced here: 214 us
  waiting for transfers between devices  88.3 us (41%)
  Pallas kernels  58.4 us (27%)
  blocking collectives  41 us (19%)
  between operations  13.4 us (6%)
  starting transfers between devices  9.42 us (4%)
    all_to_all x1, waiting for transfers between devices, body(): lax.all_to_all(terms.reshape(n_tp, rows // n_tp, full), 'tp', 0, 0, tiled...  88.3 us
    all_to_all x1, blocking collectives, body(): packed = lax.all_to_all(packed, 'sp', 0, 0, tiled=True)  22.1 us
    pallas_call x1, Pallas kernels, mixer(): pl.pallas_call(mixer_kernel, grid=(n_tp * per,), in_specs=[pl.BlockSpec((...  19 us
    all_to_all x1, blocking collectives, body(): sent = lax.all_to_all(finished, 'tp', 0, 0, tiled=True)  18.9 us
    pallas_call x2, Pallas kernels, intra(): pl.pallas_call(intra_kernel, grid=(rows // CHUNK,), in_specs=[spec(width)...  16.8 us
    pallas_call x1, Pallas kernels, project(): pl.pallas_call(project_kernel, grid=(blocks,), in_specs=[spec(a) for a in...  11.3 us
    all_to_all x1, starting transfers between devices, body(): lax.all_to_all(terms.reshape(n_tp, rows // n_tp, full), 'tp', 0, 0, tiled...  5.16 us
    pallas_call x1, Pallas kernels, local_state(): pl.pallas_call(state_kernel, out_shape=jax.ShapeDtypeStruct((slices, stat...  4.84 us
  transfers between devices with their start and end apart: 3, of which 1 were waited for; matrix products, arithmetic and copies ran while one was open for 0% of the time, Pallas kernels for 18%

profile of v1, /device:TPU:0, one launch (start us, length us, event | category | flops | bytes accessed | tf_op | source)
XLA Modules:
  0.0 214.0 jit_solution(18187240719789838707)
XLA Ops:
  6.5 0.0 all-gather.3.cloned.1.call-start
  6.5 1.7 pad_maximum_fusion
  8.2 0.0 all-gather.3.cloned.1.call-update
  8.2 4.8 %local_state.1 = bf16[32,24,384]{2,1,0:T(8,128)(2,1)} custom-call(bf16[1024,256]{1,0:T(8,128)(2,1)} %kw.1, bf16[1024,256]{1,0:T(8,128)(2,1)} %dw.1, bf16[1024,512]{1,0:T(8,128)(2,1)} %vw.1, bf16[1024,128]{1,0:T(8,128)(2,1)} %kn.1, bf16[1024,128]{1,0:T(8,128)(2,1)} %dn.1, bf16[1024,512]{1,0:T(8,128)(2,1)} %vn.1), custom_call_target="tpu_custom_call" | custom-call | tf_op jit(solution)/shard_map/local_state/pallas_call | solution.py:76
  13.1 22.1 %all_to_all.20.packed = bf16[32,24,384]{2,1,0:T(8,128)(2,1)} all-to-all(bf16[32,24,384]{2,1,0:T(8,128)(2,1)} %local_state.1), channel_id=1, replica_groups=mesh['sp'=32,'tp'=4] {'sp'}, dimensions={0} | all-to-all | bytes 1179648 | tf_op jit(solution)/shard_map/all_to_all | solution.py:306
  35.2 2.0 scan_states.1
  37.1 4.3 %all-to-all-start.1 = ((bf16[32,16,384]{2,1,0:T(8,128)(2,1)}), bf16[32,16,384]{2,1,0:T(8,128)(2,1)S(1)}, u32[]{:S(2)}, u32[]{:S(2)}) async-start(bf16[32,16,384]{2,1,0:T(8,128)(2,1)} %scan_states.1), calls=%async_computation.1 | async-start | bytes 786432 | tf_op jit(solution)/shard_map/all_to_all | solution.py:311
  41.4 8.8 %intra_wide.1 = (f32[1024,512]{1,0:T(8,128)}, bf16[1024,256]{1,0:T(8,128)(2,1)}) custom-call(bf16[1024,256]{1,0:T(8,128)(2,1)} %q.2, bf16[1024,256]{1,0:T(8,128)(2,1)} %kw.1, bf16[1024,512]{1,0:T(8,128)(2,1)} %vw.1, bf16[1024,256]{1,0:T(8,128)(2,1)} %dw.1), custom_call_target="tpu_custom_call" | custom-call | tf_op jit(solution)/shard_map/intra_wide/pallas_call | solution.py:140
  50.2 8.0 %intra_narrow.1 = (f32[1024,512]{1,0:T(8,128)}, bf16[1024,128]{1,0:T(8,128)(2,1)}) custom-call(bf16[1024,128]{1,0:T(8,128)(2,1)} %q.3, bf16[1024,128]{1,0:T(8,128)(2,1)} %kn.1, bf16[1024,512]{1,0:T(8,128)(2,1)} %vn.1, bf16[1024,128]{1,0:T(8,128)(2,1)} %dn.1), custom_call_target="tpu_custom_call" | custom-call | tf_op jit(solution)/shard_map/intra_narrow/pallas_call | solution.py:140
  58.2 0.0 all-to-all-done.1
  58.2 0.0 copy-start
  58.2 0.8 copy-done
  59.0 11.3 %project.1 = bf16[1024,2048]{1,0:T(8,128)(2,1)} custom-call(f32[1024,512]{1,0:T(8,128)} %get-tuple-element.11.aw, bf16[1024,256]{1,0:T(8,128)(2,1)} %get-tuple-element.12.cw, bf16[1024,512]{1,0:T(8,128)(2,1)} %gw.1, f32[1024,512]{1,0:T(8,128)} %get-tuple-element.13.an, bf16[1024,128]{1,0:T(8,128)(2,1)} %get-tuple-element.14.cn, bf16[1024,512]{1,0:T(8,128)(2,1)} %gn.1, ...), custom_call_target="tpu_custom_call" | custom-call | tf_op jit(solution)/shard_map/project/pallas_call | solution.py:180
  70.2 5.2 %all-to-all-start.2 = ((bf16[4,256,2048]{2,1,0:T(8,128)(2,1)}), bf16[4,256,2048]{2,1,0:T(8,128)(2,1)}, u32[]{:S(2)}, u32[]{:S(2)}) async-start(bf16[4,256,2048]{2,1,0:T(8,128)(2,1)} %bitcast.10), calls=%async_computation.2 | async-start | bytes 8388608 | tf_op jit(solution)/shard_map/all_to_all | solution.py:326
  75.4 88.3 %all-to-all-done.2.parts = bf16[4,256,2048]{2,1,0:T(8,128)(2,1)} async-done(((bf16[4,256,2048]{2,1,0:T(8,128)(2,1)}), bf16[4,256,2048]{2,1,0:T(8,128)(2,1)}, u32[]{:S(2)}, u32[]{:S(2)}) %all-to-all-start.2) | async-done | bytes 4194336 | tf_op jit(solution)/shard_map/all_to_all | solution.py:326
  163.7 4.6 %make_stream.1 = (bf16[256,2048]{1,0:T(8,128)(2,1)}, bf16[256,2048]{1,0:T(8,128)(2,1)}) custom-call(s32[1]{0:T(128)} %bitcast.place, bf16[4,256,2048]{2,1,0:T(8,128)(2,1)} %all-to-all-done.2.parts, bf16[1024,2048]{1,0:T(8,128)(2,1)} %residual.1, f32[1,2048]{1,0:T(1,128)} %bitcast.14), custom_call_target="tpu_custom_call" | custom-call | tf_op jit(solution)/shard_map/make_stream/pallas_call | solution.py:206
  168.3 0.0 all-gather.3.cloned.1.call-done
  168.3 19.0 %mixer.1 = bf16[4,256,512]{2,1,0:T(8,128)(2,1)} custom-call(bf16[256,2048]{1,0:T(8,128)(2,1)} %get-tuple-element.15.normed, bf16[256,2048]{1,0:T(8,128)(2,1)} %get-tuple-element.16.stream, bf16[32,4,128,1024]{3,2,1,0:T(8,128)(2,1)} %bitcast.8, bf16[32,4,128,1024]{3,2,1,0:T(8,128)(2,1)} %bitcast.9), custom_call_target="tpu_custom_call" | custom-call | tf_op jit(solution)/shard_map/mixer/pallas_call | solution.py:261
  187.3 18.9 %all_to_all.21 = bf16[4,256,512]{2,1,0:T(8,128)(2,1)S(1)} all-to-all(bf16[4,256,512]{2,1,0:T(8,128)(2,1)} %mixer.1), channel_id=1, replica_groups=mesh['sp'=32,'tp'=4] {'tp'}, dimensions={0} | all-to-all | bytes 2097152 | tf_op jit(solution)/shard_map/all_to_all | solution.py:330
  206.2 1.0 copy.19
Async XLA Ops:
  6.5 161.8 %all-gather.3.cloned.1.call-start = ((), (), s32[]{:S(2)}) async-start(), calls=%async_computation.4 | async-start | bytes 33816576 | tf_op jit(solution)/shard_map/all_gather | solution.py:301
  37.1 21.0 %all-to-all-start.1 = ((bf16[32,16,384]{2,1,0:T(8,128)(2,1)}), bf16[32,16,384]{2,1,0:T(8,128)(2,1)S(1)}, u32[]{:S(2)}, u32[]{:S(2)}) async-start(bf16[32,16,384]{2,1,0:T(8,128)(2,1)} %scan_states.1), calls=%async_computation.1 | async-start | bytes 786432 | tf_op jit(solution)/shard_map/all_to_all | solution.py:311
  58.2 0.8 copy-start
  70.2 93.5 %all-to-all-start.2 = ((bf16[4,256,2048]{2,1,0:T(8,128)(2,1)}), bf16[4,256,2048]{2,1,0:T(8,128)(2,1)}, u32[]{:S(2)}, u32[]{:S(2)}) async-start(bf16[4,256,2048]{2,1,0:T(8,128)(2,1)} %bitcast.10), calls=%async_computation.2 | async-start | bytes 8388608 | tf_op jit(solution)/shard_map/all_to_all | solution.py:326
Sparse Core Ops, SparseCore 0:
  10.5 148.5 all-gather.2
